TPU v7x, 32 devices: a whole 2x2x4 slice. The times are simulated.
32 devices in a mesh: sp: 8 (over z, y), tp: 4 (over x, core).
Axes of the slice: x: 2, y: 2, z: 4, core: 2. Of those that a mesh axis runs over, the one named last changes fastest.
Arguments:
- stream: bfloat16 [1024, 2048], P('sp', 'tp'), may hold values from -40 to 40
- queries: bfloat16 [1024, 1024], P('sp', 'tp'), may hold values from -6 to 6
- keys: bfloat16 [1024, 1024], P('sp', 'tp'), may hold values from -6 to 6
- values: bfloat16 [1024, 2048], P('sp', 'tp'), may hold values from -25 to 25
- out_gate: bfloat16 [1024, 2048], P('sp', 'tp'), may hold values from -8 to 8
- input_gate: float32 [1024, 8], P('sp', 'tp'), may hold values from -9 to 350
- forget_gate: float32 [1024, 8], P('sp', 'tp'), may hold values from -4 to 20
- head_gain: float32 [2048], P('tp'), may hold values from 0.1 to 1.9
- w_out: bfloat16 [2048, 2048], P('tp'), may hold values from -0.125 to 0.125
- ffn_gain: float32 [2048], replicated, may hold values from 0.1 to 1.9
- w_gate: bfloat16 [2048, 5632], P('sp', 'tp'), may hold values from -0.125 to 0.125
- w_up: bfloat16 [2048, 5632], P('sp', 'tp'), may hold values from -0.125 to 0.125
- w_down: bfloat16 [5632, 2048], P('tp', 'sp'), may hold values from -0.078125 to 0.078125
Outputs:
- mixed: bfloat16 [1024, 2048], P('sp', 'tp')
All inputs are finite; a program needn't handle non-finite values.
Results may differ from a plain program's by a relative error of at most 0.0095.
Values may be sent and summed in bfloat16 or wider, within the bound.
A program may use at most 128 MiB of HBM per device.

v0:
```python
import jax
import jax.numpy as jnp
from jax import lax
from jax.sharding import PartitionSpec as P

D = 2048
DQK = 128
DV = 256
BLOCK = 64
VALS = 2048


precise = lax.Precision.HIGHEST
norm_eps = 1e-06
very_low = -1e30


def entering(value, axis, join, neutral):
    count, mine = (lax.axis_size(axis), lax.axis_index(axis))
    pieces = jax.tree.map(lambda part: lax.all_gather(part, axis), value)
    subtotal = jax.tree.map(
        lambda part, zero: jnp.full_like(part, 0) + jnp.asarray(zero, part.dtype), value, neutral
    )

    def step(position, subtotal):
        longer = join(subtotal, jax.tree.map(lambda part: part[position], pieces))
        return jax.tree.map(lambda new, old: jnp.where(position < mine, new, old), longer, subtotal)

    return lax.fori_loop(0, count - 1, step, subtotal)


def block_summary(key_blk, value_blk, input_blk, decay_sum):
    decay_total = decay_sum[..., -1]
    log_weight = decay_total[..., None] - decay_sum + input_blk
    weight_peak = jnp.max(log_weight, axis=-1)
    weights = jnp.exp(log_weight - weight_peak[..., None])
    state_mat = jnp.einsum(
        "...ld,...le->...de", weights[..., None] * key_blk, value_blk, precision=precise
    )
    state_vec = jnp.einsum("...l,...ld->...d", weights, key_blk, precision=precise)
    return (state_mat, state_vec, weight_peak, decay_total)


def combine(earlier, later):
    ceiling = jnp.maximum(later[3] + earlier[2], later[2])
    former = jnp.exp(later[3] + earlier[2] - ceiling)
    latter = jnp.exp(later[2] - ceiling)
    return (
        former[..., None, None] * earlier[0] + latter[..., None, None] * later[0],
        former[..., None] * earlier[1] + latter[..., None] * later[1],
        ceiling,
        earlier[3] + later[3],
    )


def block_output(
    query_blk, key_blk, value_blk, input_blk, decay_sum, state_mat, state_vec, state_peak
):
    block_len = query_blk.shape[-2]
    causal = jnp.tril(jnp.ones((block_len, block_len), jnp.bool_))
    log_pair = jnp.where(
        causal,
        decay_sum[..., :, None] - decay_sum[..., None, :] + input_blk[..., None, :],
        -jnp.inf,
    )
    log_carry = decay_sum + state_peak[..., None]
    row_peak = jnp.maximum(log_carry, jnp.max(log_pair, axis=-1))
    scores = jnp.einsum("...ld,...sd->...ls", query_blk, key_blk, precision=precise) * jnp.exp(
        log_pair - row_peak[..., None]
    )
    carried = jnp.exp(log_carry - row_peak)
    numer = jnp.einsum("...ls,...se->...le", scores, value_blk, precision=precise) + carried[
        ..., None
    ] * jnp.einsum("...ld,...de->...le", query_blk, state_mat, precision=precise)
    normer = jnp.sum(scores, axis=-1) + carried * jnp.einsum(
        "...ld,...d->...l", query_blk, state_vec, precision=precise
    )
    denom = jnp.maximum(jnp.abs(normer), jnp.exp(-row_peak))
    return numer / denom[..., None]


def local(
    stream,
    queries,
    keys,
    values,
    out_gate,
    input_gate,
    forget_gate,
    head_gain,
    w_out,
    ffn_gain,
    w_gate,
    w_up,
    w_down,
):
    gate_full, up_full, down_full = (
        lax.all_gather(w_gate, "sp", axis=0, tiled=True),
        lax.all_gather(w_up, "sp", axis=0, tiled=True),
        lax.all_gather(w_down, "sp", axis=1, tiled=True),
    )
    count_of_rows = stream.shape[0]
    head_count = input_gate.shape[1]
    blocks = count_of_rows // BLOCK

    def to_blocks(array, col_width):
        return (
            array.astype(jnp.float32)
            .reshape(blocks, BLOCK, head_count, col_width)
            .transpose(2, 0, 1, 3)
        )

    query_blk = to_blocks(queries, DQK) * DQK ** (-0.5)
    key_blk = to_blocks(keys, DQK)
    value_blk = to_blocks(values, DV)
    input_blk = input_gate.reshape(blocks, BLOCK, head_count).transpose(2, 0, 1)
    decay_sum = jnp.cumsum(
        jax.nn.log_sigmoid(forget_gate).reshape(blocks, BLOCK, head_count).transpose(2, 0, 1),
        axis=-1,
    )
    summary = block_summary(key_blk, value_blk, input_blk, decay_sum)
    identity = (
        jnp.zeros((head_count, DQK, DV), jnp.float32),
        jnp.zeros((head_count, DQK), jnp.float32),
        jnp.full((head_count,), very_low, jnp.float32),
        jnp.zeros((head_count,), jnp.float32),
    )

    def advance(carry, piece):
        return (combine(carry, piece), carry)

    local_total, prefix = lax.scan(
        advance, identity, jax.tree.map(lambda array: jnp.moveaxis(array, 1, 0), summary)
    )
    carry_in = entering(local_total, "sp", combine, identity)
    start = combine(
        jax.tree.map(lambda array: array[:, None], carry_in),
        jax.tree.map(lambda array: jnp.moveaxis(array, 0, 1), prefix),
    )
    mixed_heads = block_output(
        query_blk, key_blk, value_blk, input_blk, decay_sum, start[0], start[1], start[2]
    )
    head_rows = mixed_heads.transpose(1, 2, 0, 3).reshape(count_of_rows, head_count, DV)
    local_sq = jnp.sum(head_rows * head_rows, axis=(1, 2))
    total_sq = lax.psum(local_sq, "tp")
    row_scale = lax.rsqrt(total_sq / VALS + norm_eps)
    gated = (
        head_rows
        * row_scale[:, None, None]
        * head_gain.reshape(head_count, DV)
        * jax.nn.sigmoid(out_gate.astype(jnp.float32).reshape(count_of_rows, head_count, DV))
    )
    heads_out = gated.reshape(count_of_rows, head_count * DV).astype(jnp.bfloat16)
    partial_value = jnp.dot(heads_out, w_out, preferred_element_type=jnp.float32)
    col_width = stream.shape[1]
    col_start = lax.axis_index("tp") * col_width
    mixer_own = lax.psum_scatter(
        partial_value.astype(jnp.bfloat16), "tp", scatter_dimension=1, tiled=True
    ).astype(jnp.float32)
    resid_own = (stream.astype(jnp.float32) + mixer_own).astype(jnp.bfloat16)
    resid_f = resid_own.astype(jnp.float32)
    square_total = lax.psum(jnp.sum(resid_f * resid_f, axis=-1), "tp")
    gain_own = lax.dynamic_slice_in_dim(ffn_gain, col_start, col_width)
    normed_own = (resid_f * lax.rsqrt(square_total / D + norm_eps)[:, None] * gain_own).astype(
        jnp.bfloat16
    )
    normed = lax.all_gather(normed_own, "tp", axis=1, tiled=True)
    gate_act = jnp.dot(normed, gate_full, preferred_element_type=jnp.float32)
    up_act = jnp.dot(normed, up_full, preferred_element_type=jnp.float32)
    hidden = (jax.nn.silu(gate_act) * up_act).astype(jnp.bfloat16)
    term = jnp.dot(hidden, down_full, preferred_element_type=jnp.float32)
    down_own = lax.psum_scatter(
        term.astype(jnp.bfloat16), "tp", scatter_dimension=1, tiled=True
    ).astype(jnp.float32)
    return (resid_own.astype(jnp.float32) + down_own).astype(jnp.bfloat16)


def solution(mesh):
    in_specs = (
        P("sp", "tp"),
        P("sp", "tp"),
        P("sp", "tp"),
        P("sp", "tp"),
        P("sp", "tp"),
        P("sp", "tp"),
        P("sp", "tp"),
        P("tp"),
        P("tp", None),
        P(),
        P("sp", "tp"),
        P("sp", "tp"),
        P("tp", "sp"),
    )
    out_specs = P("sp", "tp")
    return jax.shard_map(local, mesh=mesh, in_specs=in_specs, out_specs=out_specs, check_vma=False)
```

profile of v0, /device:TPU:0, one launch (start us, length us, event | category | flops | bytes accessed | tf_op | source)
XLA Modules:
  0.0 422.1 jit_solution(10034435100602329406)
XLA Ops:
  6.6 0.8 fusion.59
  7.5 0.5 reduce_window_sum.13
  8.2 0.8 reshape.66
  9.2 0.9 reshape.64
  10.0 0.9 reshape.67
  11.0 0.5 convolution_bitcast_fusion
  11.5 0.2 fusion.46
  11.8 2.2 while.43
  11.9 0.8 bitcast_dynamic-update-slice_fusion.2
  13.0 0.7 bitcast_dynamic-update-slice_fusion.2
  14.0 0.7 copy-done.1
  14.8 0.6 dynamic-slice
  16.1 0.2 dynamic-update-slice
  16.3 0.2 dynamic-update-slice.1
  16.5 23.2 %all-reduce.2 = (f32[16]{0:T(128)S(1)}, f32[16]{0:T(128)S(1)}) all-reduce(f32[16]{0:T(128)S(1)} %dynamic-update-slice, f32[16]{0:T(128)S(1)} %dynamic-update-slice.1), channel_id=2, replica_groups=mesh['sp'=8,'tp'=4] {'sp'}, use_global_device_ids=true, to_apply=%add | all-reduce | flops 32 | bytes 256
  40.0 16.7 %all-gather.4 = f32[8,2,128]{2,1,0:T(2,128)S(1)} all-gather(f32[1,2,128]{2,1,0:T(2,128)S(1)} %bitcast.218), channel_id=5, replica_groups=mesh['sp'=8,'tp'=4] {'sp'}, dimensions={0}, use_global_device_ids=true | all-gather | bytes 9216 | tf_op jit(solution)/shard_map/all_gather | solution.py:20
  56.8 10.0 %all-gather.16.cloned.1.call-done = f32[16,128,256]{2,1,0:T(8,128)} async-done(((f32[2,128,256]{2,1,0:T(8,128)}), f32[16,128,256]{2,1,0:T(8,128)}) %all-gather.16.cloned.1.call-update) | async-done | bytes 2097168 | tf_op jit(solution)/shard_map/all_gather | solution.py:20
  66.8 8.3 %while.44 = (s32[]{:T(128)}, f32[2,128,256]{2,1,0:T(8,128)S(1)}, f32[2,128]{1,0:T(2,128)S(1)}, f32[2]{0:T(128)S(1)}, s32[]{:T(128)}, /*index=5*/f32[8,2]{1,0:T(8...) while((s32[]{:T(128)}, f32[2,128,256]{2,1,0:T(8,128)S(1)}, ...), condition=%wide.region_5.6_spmd.clone, body=%wide.region_4.5_spmd.clone.sunk | while | flops 328978 | bytes 789757 | solution.py:29
  66.9 1.1 fusion.87
  68.1 1.1 fusion.87
  69.2 1.1 fusion.87
  70.4 1.1 fusion.87
  71.6 1.1 fusion.87
  72.8 1.1 fusion.87
  74.0 1.1 fusion.87
  75.3 0.3 fusion.67
  75.6 0.3 convolution_bitcast_fusion.2
  76.0 0.3 fusion.31
  76.5 1.7 multiply_reduce_fusion
  78.2 0.2 copy.45
  78.5 5.6 %psum.14 = f32[128]{0:T(128)S(1)} all-reduce(f32[128]{0:T(128)S(1)} %reduce_sum.34), channel_id=1, replica_groups=mesh['sp'=8,'tp'=4] {'tp'}, use_global_device_ids=true, to_apply=%region_9.10 | all-reduce | flops 128 | bytes 1024 | tf_op jit(solution)/shard_map/psum | solution.py:145
  84.2 1.3 convolution_convert_fusion
  85.6 0.7 all-gather.10.cloned.1.call-update
  86.3 0.5 all-gather.12.cloned.1.call-update
  86.9 0.5 all-gather.14.cloned.1.call-update
  87.5 0.8 dynamic_slice.46
  88.2 17.9 %reduce-scatter.3.cloned.1.call-done = bf16[128,512]{1,0:T(8,128)(2,1)} async-done(((bf16[128,2048]{1,0:T(8,128)(2,1)}), bf16[128,512]{1,0:T(8,128)(2,1)}) %reduce-scatter.3.cloned.1.call-update) | async-done | bytes 131088 | tf_op jit(solution)/shard_map/reduce_scatter | solution.py:157
  106.1 1.0 fusion.25
  107.1 5.8 %psum.15 = f32[128]{0:T(128)S(1)} all-reduce(f32[128]{0:T(128)S(1)} %fusion.25), channel_id=1, replica_groups=mesh['sp'=8,'tp'=4] {'tp'}, use_global_device_ids=true, to_apply=%region_12.13 | all-reduce | flops 128 | bytes 1024 | tf_op jit(solution)/shard_map/psum | solution.py:162
  112.9 1.0 fusion.27
  113.9 6.9 %all_gather.44 = bf16[128,2048]{1,0:T(8,128)(2,1)S(1)} all-gather(bf16[128,512]{1,0:T(8,128)(2,1)S(1)} %fusion.27), channel_id=1, replica_groups=mesh['sp'=8,'tp'=4] {'tp'}, dimensions={1}, use_global_device_ids=true | all-gather | bytes 655360 | tf_op jit(solution)/shard_map/all_gather | solution.py:167
  120.8 79.9 %all-gather.10.cloned.1.call-done = bf16[2048,1408]{1,0:T(8,128)(2,1)} async-done(((bf16[256,1408]{1,0:T(8,128)(2,1)}), bf16[2048,1408]{1,0:T(8,128)(2,1)}) %all-gather.10.cloned.1.call-update) | async-done | bytes 5767184 | tf_op jit(solution)/shard_map/all_gather | solution.py:98
  200.7 4.5 %fusion.68 = f32[128,1408]{1,0:T(8,128)} fusion(bf16[128,2048]{1,0:T(8,128)(2,1)S(1)} %all_gather.44, bf16[2048,1408]{1,0:T(8,128)(2,1)} %all-gather.10.cloned.1.call-done), kind=kOutput, calls=%fused_computation.119 | convolution fusion | flops 738197504 | bytes 7012352 | tf_op jit(solution)/shard_map/dot_general | solution.py:168
  205.2 88.0 %all-gather.12.cloned.1.call-done = bf16[2048,1408]{1,0:T(8,128)(2,1)} async-done(((bf16[256,1408]{1,0:T(8,128)(2,1)}), bf16[2048,1408]{1,0:T(8,128)(2,1)}) %all-gather.12.cloned.1.call-update) | async-done | bytes 5767184 | tf_op jit(solution)/shard_map/all_gather | solution.py:99
  293.2 93.2 %all-gather.14.cloned.1.call-done = bf16[1408,2048]{1,0:T(8,128)(2,1)} async-done(((bf16[1408,256]{1,0:T(8,128)(2,1)}), bf16[1408,2048]{1,0:T(8,128)(2,1)}) %all-gather.14.cloned.1.call-update) | async-done | bytes 5767184 | tf_op jit(solution)/shard_map/all_gather | solution.py:100
  386.5 7.2 %convolution_convert_fusion.1 = bf16[128,2048]{1,0:T(8,128)(2,1)} fusion(bf16[1408,2048]{1,0:T(8,128)(2,1)} %all-gather.14.cloned.1.call-done, bf16[128,2048]{1,0:T(8,128)(2,1)S(1)} %all_gather.44, bf16[2048,1408]{1,0:T(8,128)(2,1)} %all-gather.12.cloned.1.call-done, f32[128,1408]{1,0:T(8,128)} %fusion.68), kind=kOutput, calls=%fused_computation.40 | convolution fusion | flops 1477738496 | bytes 13303808 | tf_op jit(solution)/shard_map/dot_general | solution.py:171
  393.7 20.0 %reduce-scatter.5.cloned.1.call-done = bf16[128,512]{1,0:T(8,128)(2,1)} async-done(((bf16[128,2048]{1,0:T(8,128)(2,1)}), bf16[128,512]{1,0:T(8,128)(2,1)}) %reduce-scatter.5.cloned.1.call-update) | async-done | bytes 131088 | tf_op jit(solution)/shard_map/reduce_scatter | solution.py:172
  413.7 1.6 fusion.28
  (99 shorter events, 3.3 us)
Async XLA Ops:
  6.5 77.6 %copy-start = (bf16[512,2048]{1,0:T(8,128)(2,1)S(1)}, bf16[512,2048]{1,0:T(8,128)(2,1)}, u32[]{:S(2)}) copy-start(bf16[512,2048]{1,0:T(8,128)(2,1)} %param.25) | copy-start | bytes 6291460
  6.5 8.3 %copy-start.7 = (u32[32]{0:T(128)S(1)}, u32[32]{0:T(128)}, u32[]{:S(2)}) copy-start(u32[32]{0:T(128)} %constant.93) | copy-start | bytes 388
  6.5 33.4 %copy-start.4 = (bf16[128,256]{1,0:T(8,128)(2,1)S(1)}, bf16[128,256]{1,0:T(8,128)(2,1)}, u32[]{:S(2)}) copy-start(bf16[128,256]{1,0:T(8,128)(2,1)} %param.18) | copy-start | bytes 196612
  6.5 60.3 %all-gather.16.cloned.1.call-start = ((), (), s32[]{:S(2)}) async-start(), calls=%async_computation.7 | async-start | bytes 2359296 | tf_op jit(solution)/shard_map/all_gather | solution.py:20
  14.0 0.7 copy-start.1
  14.0 70.2 %copy-start.5 = (bf16[128,512]{1,0:T(8,128)(2,1)S(1)}, bf16[128,512]{1,0:T(8,128)(2,1)}, u32[]{:S(2)}) copy-start(bf16[128,512]{1,0:T(8,128)(2,1)} %param.21) | copy-start | bytes 393220
  14.0 70.1 %copy-start.6 = (f32[512]{0:T(512)S(1)}, f32[512]{0:T(512)}, u32[]{:S(2)}) copy-start(f32[512]{0:T(512)} %param.24) | copy-start | bytes 6148
  14.7 91.4 %reduce-scatter.3.cloned.1.call-start = ((), (), s32[]{:S(2)}) async-start(), calls=%async_computation.2 | async-start | bytes 655360 | tf_op jit(solution)/shard_map/reduce_scatter | solution.py:157
  75.1 31.0 %copy-start.2 = (bf16[128,512]{1,0:T(8,128)(2,1)S(1)}, bf16[128,512]{1,0:T(8,128)(2,1)}, u32[]{:S(2)}) copy-start(bf16[128,512]{1,0:T(8,128)(2,1)} %param.17) | copy-start | bytes 393220
  85.5 115.2 %all-gather.10.cloned.1.call-start = ((), (), s32[]{:S(2)}) async-start(), calls=%async_computation.3 | async-start | bytes 6488064 | tf_op jit(solution)/shard_map/all_gather | solution.py:98
  86.2 207.0 %all-gather.12.cloned.1.call-start = ((), (), s32[]{:S(2)}) async-start(), calls=%async_computation.4 | async-start | bytes 6488064 | tf_op jit(solution)/shard_map/all_gather | solution.py:99
  86.8 299.6 %all-gather.14.cloned.1.call-start = ((), (), s32[]{:S(2)}) async-start(), calls=%async_computation.5 | async-start | bytes 6488064 | tf_op jit(solution)/shard_map/all_gather | solution.py:100
  87.4 326.3 %reduce-scatter.5.cloned.1.call-start = ((), (), s32[]{:S(2)}) async-start(), calls=%async_computation.6 | async-start | bytes 655360 | tf_op jit(solution)/shard_map/reduce_scatter | solution.py:172
  205.2 208.5 %copy-start.3 = (bf16[128,512]{1,0:T(8,128)(2,1)S(1)}, bf16[128,512]{1,0:T(8,128)(2,1)}, u32[]{:S(2)}) copy-start(bf16[128,512]{1,0:T(8,128)(2,1)} %reduce-scatter.3.cloned.1.call-done) | copy-start | bytes 393220
Sparse Core Ops, SparseCore 0:
  14.9 51.9 all-gather.15
  85.6 20.4 reduce-scatter.2
  108.3 92.3 all-gather.9
  202.7 90.4 all-gather.11
  295.1 91.2 all-gather.13
  393.8 19.7 reduce-scatter.4
where the time goes:
time: 423 us; the launch traced here: 422 us
  waiting for transfers between devices  311 us (74%)
  blocking collectives  58.2 us (14%)
  matrix products  16.3 us (4%)
  other arithmetic  15.8 us (4%)
  between operations  14.4 us (3%)
  local copies, waits for them, and re-layouts  6.37 us (2%)
    all_gather x1, waiting for transfers between devices, local(): lax.all_gather(w_down, 'sp', axis=1, tiled=True)  93.2 us
    all_gather x1, waiting for transfers between devices, local(): lax.all_gather(w_up, 'sp', axis=0, tiled=True)  88 us
    all_gather x1, waiting for transfers between devices, local(): lax.all_gather(w_gate, 'sp', axis=0, tiled=True)  79.9 us
    unnamed x1, blocking collectives  23.2 us
    reduce_scatter x1, waiting for transfers between devices, local(): lax.psum_scatter(term.astype(jnp.bfloat16), 'tp', scatter_dimension=1, ti...  20 us
    reduce_scatter x1, waiting for transfers between devices, local(): lax.psum_scatter(partial_value.astype(jnp.bfloat16), 'tp', scatter_dimens...  17.9 us
    all_gather x1, blocking collectives, entering(): pieces = jax.tree.map(lambda part: lax.all_gather(part, axis), value)  16.7 us
    all_gather x1, waiting for transfers between devices, entering(): pieces = jax.tree.map(lambda part: lax.all_gather(part, axis), value)  10 us
  transfers between devices with their start and end apart: 6, of which 6 were waited for; matrix products, arithmetic and copies ran while one was open for 2% of the time, Pallas kernels for 0%

commit v1 on v0

--- a/solution.py
+++ b/solution.py
@@ -1,6 +1,10 @@
+import functools
+
 import jax
 import jax.numpy as jnp
 from jax import lax
+from jax.experimental import pallas as pl
+from jax.experimental.pallas import tpu as pltpu
 from jax.sharding import PartitionSpec as P
 
 D = 2048
@@ -175,6 +179,412 @@
     return (resid_own.astype(jnp.float32) + down_own).astype(jnp.bfloat16)
 
 
+def exclusive(a, b, count):
+    total, bit = 0, 1
+    while bit < count:
+        total = total + bit * ((a // bit + b // bit) % 2)
+        bit *= 2
+    return total
+
+
+def remote(src, dst, send, recv, target):
+    return pltpu.make_async_remote_copy(
+        src_ref=src,
+        dst_ref=dst,
+        send_sem=send,
+        recv_sem=recv,
+        device_id=target,
+        device_id_type=pl.DeviceIdType.MESH,
+    )
+
+
+def fused_kernel(
+    n, m, heads, stream_ref, q_ref, kv_ref, og_ref, g_ref, hg_ref, wo_ref, fg_ref, wgu_ref, wd_ref,
+    out_ref, kvb, gb, wgub, wdb, xb, ob, sqb, ry, rz, rbs, sems,
+):
+    rows, width = stream_ref.shape
+    levels = len(rbs)
+    dv = width // heads
+    dqk = q_ref.shape[1] // heads
+    s, t = lax.axis_index("sp"), lax.axis_index("tp")
+    sp_at = lambda r: exclusive(s, r, n)
+    tp_at = lambda r: exclusive(t, r, m)
+    to_sp = lambda r: (sp_at(r), t)
+    to_tp = lambda r: (s, tp_at(r))
+
+    barrier = pltpu.get_barrier_semaphore()
+    for r in range(1, n):
+        pl.semaphore_signal(barrier, inc=1, device_id=to_sp(r), device_id_type=pl.DeviceIdType.MESH)
+    for r in range(1, m):
+        pl.semaphore_signal(barrier, inc=1, device_id=to_tp(r), device_id_type=pl.DeviceIdType.MESH)
+    pl.semaphore_wait(barrier, n + m - 2)
+
+    def kv_copy(r):
+        return remote(kv_ref, kvb.at[s], sems["kv_s"].at[r], sems["kv_r"].at[r], to_sp(r))
+
+    def kv_forward(r):
+        piece = kvb.at[sp_at(r)]
+        return remote(piece, piece, sems["kvf_s"].at[r], sems["kv_r"].at[r + 1], to_sp(1))
+
+    def g_copy(r):
+        return remote(g_ref, gb.at[s], sems["g_s"].at[r], sems["g_r"].at[r], to_sp(r))
+
+    def gu_copy(r):
+        return remote(
+            wgu_ref.at[sp_at(r)], wgub.at[s], sems["gu_s"].at[r], sems["gu_r"].at[r], to_sp(r)
+        )
+
+    def d_copy(r):
+        return remote(wd_ref.at[sp_at(r)], wdb.at[s], sems["d_s"].at[r], sems["d_r"].at[r], to_sp(r))
+
+    def sq_copy(r):
+        return remote(sqb.at[t], sqb.at[t], sems["sq_s"].at[r], sems["sq_r"].at[r], to_tp(r))
+
+    def x_copy(r):
+        piece = xb.at[s, t]
+        return remote(piece, piece, sems["x_s"].at[r], sems["x_r"].at[r], to_sp(r))
+
+    def x_forward(r):
+        piece = xb.at[sp_at(r), t]
+        return remote(piece, piece, sems["xf_s"].at[r], sems["x_r"].at[r + 1], to_sp(1))
+
+    def xt_copy(level, r, j):
+        span = 2 << level
+        piece = xb.at[sp_at(r), t % span + j * span]
+        return remote(
+            piece, piece, sems["xt_s"].at[level, r, j], sems["xt_r"].at[level, r, j], to_tp(1 << level)
+        )
+
+    def rs_copy(level, b, j):
+        span = 2 << level
+        return remote(
+            ob.at[b, tp_at(1 << level) % span + j * span],
+            rbs[level].at[b, j],
+            sems["rs_s"].at[level, b, j],
+            sems["rs_r"].at[level, b, j],
+            to_tp(1 << level),
+        )
+
+    def y_copy(r):
+        return remote(ob.at[sp_at(r + 1), t], ry.at[r], sems["y_s"].at[r], sems["y_r"].at[r], to_sp(1))
+
+    def z_copy(r):
+        return remote(ob.at[sp_at(r), t], rz.at[r], sems["z_s"].at[r], sems["z_r"].at[r], to_sp(r))
+
+    share = lambda level: m >> (level + 1)
+    direct = list(range(2, n, 2)) + [1]
+    own = [
+        pltpu.make_async_copy(kv_ref, kvb.at[s], sems["own"].at[0]),
+        pltpu.make_async_copy(g_ref, gb.at[s], sems["own"].at[1]),
+        pltpu.make_async_copy(wgu_ref.at[s], wgub.at[s], sems["own"].at[2]),
+        pltpu.make_async_copy(wd_ref.at[s], wdb.at[s], sems["own"].at[3]),
+    ]
+    for r in range(1, n):
+        g_copy(r).start()
+    for r in direct:
+        kv_copy(r).start()
+    for copy in own:
+        copy.start()
+    for r in range(2, n, 2):
+        gu_copy(r).start()
+    for r in range(2, n, 2):
+        kv_copy(r).wait_recv()
+        kv_forward(r).start()
+    for r in range(1, n, 2):
+        gu_copy(r).start()
+    for r in range(1, n):
+        d_copy(r).start()
+    for r in range(1, n):
+        g_copy(r).wait_recv()
+    for r in range(1, n, 2):
+        kv_copy(r).wait_recv()
+    for copy in own:
+        copy.wait()
+
+    def rs_send(level, b):
+        for j in range(share(level)):
+            rs_copy(level, b, j).start()
+
+    def rs_add(level, b):
+        span = 2 << level
+        for j in range(share(level)):
+            rs_copy(level, b, j).wait_recv()
+            mine = t % span + j * span
+            ob[b, mine] = (
+                ob[b, mine].astype(jnp.float32) + rbs[level][b, j].astype(jnp.float32)
+            ).astype(jnp.bfloat16)
+
+    at_row = lax.broadcasted_iota(jnp.int32, (rows, rows), 0)
+    at_col = lax.broadcasted_iota(jnp.int32, (rows, rows), 1)
+    eye, causal = at_row == at_col, at_row >= at_col
+    to_column = lambda row: jnp.sum(jnp.where(eye, row, 0.0), axis=1, keepdims=True)
+    upper = (at_row <= at_col).astype(jnp.float32)
+    gates = gb[...].reshape(n * gb.shape[1], rows)
+    log_forget = jnp.minimum(gates, 0.0) - jnp.log1p(jnp.exp(-jnp.abs(gates)))
+    decays = jnp.dot(log_forget, upper, precision=precise, preferred_element_type=jnp.float32)
+    own_gate = g_ref[...]
+    own_log = jnp.minimum(own_gate, 0.0) - jnp.log1p(jnp.exp(-jnp.abs(own_gate)))
+    own_decay = jnp.dot(own_log, upper, precision=precise, preferred_element_type=jnp.float32)
+    step = gb.shape[1]
+    square = jnp.zeros((rows, 1), jnp.float32)
+    gated = []
+    for h in range(heads):
+        decay_row = own_decay[h : h + 1]
+        decay_col = to_column(decay_row)
+        after = jnp.zeros((1, 1), jnp.float32)
+        peak = jnp.full((1, 1), very_low, jnp.float32)
+        weights = [None] * n
+        for j in reversed(range(n)):
+            earlier = j < s
+            block = decays[j * step + h : j * step + h + 1]
+            total = block[:, rows - 1 :]
+            entry = gates[j * step + heads + h : j * step + heads + h + 1]
+            weights[j] = jnp.where(earlier, total - block + entry + after, very_low)
+            after = after + jnp.where(earlier, total, 0.0)
+            peak = jnp.maximum(peak, jnp.max(weights[j], axis=1, keepdims=True))
+        pair = jnp.where(causal, decay_col - decay_row + own_gate[heads + h : heads + h + 1], very_low)
+        row_peak = jnp.maximum(decay_col + peak, jnp.max(pair, axis=1, keepdims=True))
+        query = q_ref[:, h * dqk : (h + 1) * dqk]
+        numer = jnp.zeros((rows, dv), jnp.float32)
+        normer = jnp.zeros((rows, 1), jnp.float32)
+
+        def add(numer, normer, source, log_weight):
+            key = source[:, h * dqk : (h + 1) * dqk]
+            value = source[:, heads * dqk + h * dv : heads * dqk + (h + 1) * dv]
+            scores = lax.dot_general(
+                query, key, (((1,), (1,)), ((), ())), preferred_element_type=jnp.float32
+            )
+            scores = scores * dqk ** (-0.5) * jnp.exp(log_weight - row_peak)
+            high = scores.astype(jnp.bfloat16)
+            low = (scores - high.astype(jnp.float32)).astype(jnp.bfloat16)
+            numer = (
+                numer
+                + jnp.dot(high, value, preferred_element_type=jnp.float32)
+                + jnp.dot(low, value, preferred_element_type=jnp.float32)
+            )
+            return numer, normer + jnp.sum(scores, axis=1, keepdims=True)
+
+        numer, normer = add(numer, normer, kv_ref, pair)
+        for j in range(n - 1):
+            numer, normer = add(numer, normer, kvb.at[j], decay_col + weights[j])
+        cell = numer / jnp.maximum(jnp.abs(normer), jnp.exp(-row_peak))
+        square = square + jnp.sum(cell * cell, axis=1, keepdims=True)
+        spot = slice(h * dv, (h + 1) * dv)
+        gate = 1.0 / (1.0 + jnp.exp(-og_ref[:, spot].astype(jnp.float32)))
+        gated.append((cell * hg_ref[:, spot] * gate).astype(jnp.bfloat16))
+    heads_out = jnp.concatenate(gated, axis=1)
+    square_row = jnp.sum(jnp.where(eye, square, 0.0), axis=0, keepdims=True)
+    sqb[t] = jnp.broadcast_to(square_row, sqb.shape[1:])
+    for r in range(1, m):
+        sq_copy(r).start()
+    for j in range(m):
+        ob[n, j] = jnp.dot(
+            heads_out, wo_ref[:, j * width : (j + 1) * width], preferred_element_type=jnp.float32
+        ).astype(jnp.bfloat16)
+    for level in range(levels):
+        rs_send(level, n)
+        rs_add(level, n)
+    for r in range(1, m):
+        sq_copy(r).wait_recv()
+    total_sq = to_column(jnp.sum(sqb[...], axis=0)[0:1])
+    row_scale = lax.rsqrt(total_sq / (m * width) + norm_eps)
+    mixer = ob[n, t].astype(jnp.float32) * row_scale
+    xb[s, t] = (stream_ref[...].astype(jnp.float32) + mixer).astype(jnp.bfloat16)
+
+    for r in direct:
+        x_copy(r).start()
+    order = [0] + [r for base in range(2, n, 2) for r in (base, base + 1)] + [1]
+    for i in range(n + levels):
+        if i < n:
+            r = order[i]
+            if r:
+                x_copy(r).wait_recv()
+            if r and r % 2 == 0:
+                x_forward(r).start()
+            for j in range(share(levels - 1)):
+                xt_copy(levels - 1, r, j).start()
+        for back in range(1, levels + 1):
+            if 0 <= i - back < n:
+                r, level = order[i - back], levels - back
+                for j in range(share(level)):
+                    xt_copy(level, r, j).wait_recv()
+                if level:
+                    for j in range(share(level - 1)):
+                        xt_copy(level - 1, r, j).start()
+    for r in range(1, n):
+        gu_copy(r).wait_recv()
+    for r in range(1, n):
+        d_copy(r).wait_recv()
+
+    part, depth = wdb.shape[1], wgub.shape[2]
+    nt = (((1,), (1,)), ((), ()))
+
+    def relation(i):
+        return exclusive((i + 2) % n, 1, n)
+
+    def work(i, carry):
+        @pl.when(i < n)
+        def _():
+            b = sp_at(relation(i))
+            squares = jnp.zeros((rows, 1), jnp.float32)
+            for j in range(m):
+                piece = xb[b, j].astype(jnp.float32)
+                squares = squares + jnp.sum(piece * piece, axis=1, keepdims=True)
+            scale = lax.rsqrt(squares / (m * width) + norm_eps)
+            gate_act = jnp.zeros((rows, part), jnp.float32)
+            up_act = jnp.zeros((rows, part), jnp.float32)
+            per = width // depth
+            for k in range(n):
+                j, c = k // per, (k % per) * depth
+                piece = xb[b, j, :, c : c + depth].astype(jnp.float32)
+                normed = (piece * scale * fg_ref[:, k * depth : (k + 1) * depth]).astype(jnp.bfloat16)
+                gate_act += lax.dot_general(
+                    normed, wgub[k, :part], nt, preferred_element_type=jnp.float32
+                )
+                up_act += lax.dot_general(
+                    normed, wgub[k, part:], nt, preferred_element_type=jnp.float32
+                )
+            hidden = (gate_act / (1.0 + jnp.exp(-gate_act)) * up_act).astype(jnp.bfloat16)
+            for k in range(n):
+                j, c = k // per, (k % per) * depth
+                ob[b, j, :, c : c + depth] = jnp.dot(
+                    hidden, wdb[k], preferred_element_type=jnp.float32
+                ).astype(jnp.bfloat16)
+            rs_send(0, b)
+
+        for level in range(levels):
+            at = i - 1 - level
+
+            @pl.when((at >= 0) & (at < n))
+            def _():
+                r = relation(at)
+                b = sp_at(r)
+                rs_add(level, b)
+                if level + 1 < levels:
+                    rs_send(level + 1, b)
+                else:
+
+                    @pl.when(r % 2 == 1)
+                    def _():
+                        y_copy(r - 1).start()
+
+        at = i - 1 - levels
+
+        @pl.when((at >= 0) & (at < n))
+        def _():
+            r = relation(at)
+            b = sp_at(r)
+
+            @pl.when(r % 2 == 0)
+            def _():
+                y_copy(r).wait_recv()
+                ob[b, t] = (
+                    ob[b, t].astype(jnp.float32) + ry[r].astype(jnp.float32)
+                ).astype(jnp.bfloat16)
+
+                @pl.when(r > 0)
+                def _():
+                    z_copy(r).start()
+
+        return carry
+
+    lax.fori_loop(0, n + levels + 1, work, 0)
+    final = xb[s, t].astype(jnp.float32) + ob[s, t].astype(jnp.float32)
+    for r in range(2, n, 2):
+        z_copy(r).wait_recv()
+        final = final + rz[r].astype(jnp.float32)
+    out_ref[...] = final.astype(jnp.bfloat16)
+
+    for r in range(1, n):
+        g_copy(r).wait_send()
+        gu_copy(r).wait_send()
+        d_copy(r).wait_send()
+    for r in range(1, m):
+        sq_copy(r).wait_send()
+    for r in direct:
+        kv_copy(r).wait_send()
+        x_copy(r).wait_send()
+    for r in range(2, n, 2):
+        kv_forward(r).wait_send()
+        x_forward(r).wait_send()
+        z_copy(r).wait_send()
+    for r in range(0, n, 2):
+        y_copy(r).wait_send()
+    for level in range(levels):
+        for j in range(share(level)):
+            for r in range(n):
+                xt_copy(level, r, j).wait_send()
+            for b in range(n + 1):
+                rs_copy(level, b, j).wait_send()
+
+
+def fused(
+    n, m, stream, queries, keys, values, out_gate, input_gate, forget_gate, head_gain, w_out,
+    ffn_gain, w_gate, w_up, w_down,
+):
+    rows, width = stream.shape
+    heads = input_gate.shape[1]
+    depth, hidden = w_gate.shape
+    part = hidden // n
+    levels = m.bit_length() - 1
+    kv = jnp.concatenate([keys, values], axis=1)
+    gates = jnp.concatenate([forget_gate, input_gate], axis=1).T
+    gates = jnp.pad(gates, ((0, -gates.shape[0] % 8), (0, 0)))
+    flip = lambda w: w.T.reshape(n, part, depth)
+    wgu = jnp.concatenate([flip(w_gate), flip(w_up)], axis=1)
+    wd = w_down.reshape(n, part, depth)
+    piece = (rows, width)
+    low = jnp.bfloat16
+    dma = pltpu.SemaphoreType.DMA
+    pairs = ("kv", "g", "gu", "d", "x", "y", "z")
+    sems = {name + end: dma((n,)) for name in pairs for end in ("_s", "_r")}
+    sems.update(kvf_s=dma((n,)), xf_s=dma((n,)))
+    sems.update(sq_s=dma((m,)), sq_r=dma((m,)), own=dma((4,)))
+    sems.update(xt_s=dma((levels, n, m // 2)), xt_r=dma((levels, n, m // 2)))
+    sems.update(rs_s=dma((levels, n + 1, m // 2)), rs_r=dma((levels, n + 1, m // 2)))
+    vmem = pl.BlockSpec(memory_space=pltpu.VMEM)
+    return pl.pallas_call(
+        functools.partial(fused_kernel, n, m, heads),
+        out_shape=jax.ShapeDtypeStruct(piece, low),
+        in_specs=[vmem] * 10,
+        out_specs=vmem,
+        scratch_shapes=[
+            pltpu.VMEM((n,) + kv.shape, low),
+            pltpu.VMEM((n,) + gates.shape, jnp.float32),
+            pltpu.VMEM(wgu.shape, low),
+            pltpu.VMEM(wd.shape, low),
+            pltpu.VMEM((n, m) + piece, low),
+            pltpu.VMEM((n + 1, m) + piece, low),
+            pltpu.VMEM((m, 8, rows), jnp.float32),
+            pltpu.VMEM((n,) + piece, low),
+            pltpu.VMEM((n,) + piece, low),
+            [pltpu.VMEM((n + 1, m >> (level + 1)) + piece, low) for level in range(levels)],
+            sems,
+        ],
+        compiler_params=pltpu.CompilerParams(
+            collective_id=0, has_side_effects=True, vmem_limit_bytes=60 * 2**20
+        ),
+    )(
+        stream, queries, kv, out_gate, gates, head_gain.reshape(1, -1), w_out,
+        ffn_gain.reshape(1, -1), wgu, wd,
+    )
+
+
+def fits(n, m, stream, input_gate, w_gate):
+    rows, width = stream.shape
+    depth, hidden = w_gate.shape
+    powers = n & (n - 1) == 0 and m & (m - 1) == 0 and n > 1 and m > 1
+    tiled = hidden % (16 * n) == 0 and depth % 128 == 0 and width % depth == 0 and rows == 128
+    held = rows * width * 2 * n * (5 * m // 2 + 6) + 12 * depth * hidden
+    return powers and tiled and 2 * input_gate.shape[1] <= 8 and held < 40 * 2**20
+
+
+def body(n, m, *arrays):
+    if fits(n, m, arrays[0], arrays[5], arrays[10]):
+        return fused(n, m, *arrays)
+    return local(*arrays)
+
+
 def solution(mesh):
     in_specs = (
         P("sp", "tp"),
@@ -192,4 +602,5 @@
         P("tp", "sp"),
     )
     out_specs = P("sp", "tp")
-    return jax.shard_map(local, mesh=mesh, in_specs=in_specs, out_specs=out_specs, check_vma=False)
+    each = functools.partial(body, mesh.shape["sp"], mesh.shape["tp"])
+    return jax.shard_map(each, mesh=mesh, in_specs=in_specs, out_specs=out_specs, check_vma=False)

time: 423 us -> 141 us (0.33)
  waiting for transfers between devices: 311 us -> 0 us
  Pallas kernels: 0 us -> 134 us
  blocking collectives: 58.2 us -> 0 us
  matrix products: 16.3 us -> 0 us
  between operations: 14.4 us -> 0.05 us
  other arithmetic: 15.8 us -> 1.91 us
    all_gather x4 -> x0, waiting for transfers between devices: 271 us -> none  [the longest x1 93.2 us: local(): lax.all_gather(w_down, 'sp', axis=1, tiled=True)]
    pallas_call x0 -> x1, Pallas kernels: none -> 134 us  [fused(): pl.pallas_call(functools.partial(fused_kernel, n, m, heads), out_shape=ja...]
    reduce_scatter x2 -> x0, waiting for transfers between devices: 37.9 us -> none  [the longest x1 20 us: local(): lax.psum_scatter(term.astype(jnp.bfloat16), 'tp', scatter_dimension=1, ti...]
    all_gather x2 -> x0, blocking collectives: 23.5 us -> none  [the longest x1 16.7 us: entering(): pieces = jax.tree.map(lambda part: lax.all_gather(part, axis), value)]
    unnamed x1 -> x0, blocking collectives: 23.2 us -> none
    dot_general x9 -> x0, matrix products: 16.3 us -> none  [the longest x1 7.25 us: local(): term = jnp.dot(hidden, down_full, preferred_element_type=jnp.float32)]
    psum x2 -> x0, blocking collectives: 11.4 us -> none  [the longest x1 5.75 us: local(): square_total = lax.psum(jnp.sum(resid_f * resid_f, axis=-1), 'tp')]
    select_n x21 -> x0, other arithmetic: 8.15 us -> none  [step(): jnp.where(position < mine, new, old)]
  transfers between devices with their start and end apart: 6 -> 0, of which waited for: 6 -> 0; matrix products, arithmetic and copies ran while one was open for 2% -> 0% of each run, Pallas kernels for 0% -> 0%
where the time goes in v1:
time: 141 us
  Pallas kernels  134 us (95%)
  local copies, waits for them, and re-layouts  5.03 us (4%)
  other arithmetic  1.91 us (1%)
    pallas_call x1, Pallas kernels, fused(): pl.pallas_call(functools.partial(fused_kernel, n, m, heads), out_shape=ja...  134 us
    transpose x2, local copies, waits for them, and re-layouts, fused(): flip = lambda w: w.T.reshape(n, part, depth)  2.84 us

profile of v1, /device:TPU:0, one launch (start us, length us, event | category | flops | bytes accessed | tf_op | source)
XLA Modules:
  0.0 140.5 jit_solution(5564436042042623803)
XLA Ops:
  0.0 1.4 copy.14
  1.4 0.0 copy-start
  1.4 0.0 copy-start.1
  1.4 0.0 copy-start.2
  1.4 0.0 copy-start.3
  1.4 1.5 %copy.15 = bf16[1408,256]{1,0:T(8,128)(2,1)S(1)} copy(bf16[1408,256]{0,1:T(8,128)(2,1)} %bitcast.12) | data formatting | bytes 1441792 | tf_op jit(solution)/shard_map/transpose | solution.py:533
  2.9 1.2 pad_maximum_fusion.wgu_ref
  4.1 0.0 copy-done
  4.1 0.0 copy-done.1
  4.1 0.7 pad_maximum_fusion.1.kv_ref
  4.8 0.0 copy-done.2
  4.8 0.0 copy-done.3
  4.8 0.6 pad.4.g_ref
  5.4 133.5 %shard_map.127 = bf16[128,512]{1,0:T(8,128)(2,1)} custom-call(bf16[128,512]{1,0:T(8,128)(2,1)} %stream_ref.1, bf16[128,256]{1,0:T(8,128)(2,1)} %q_ref.1, bf16[128,768]{1,0:T(8,128)(2,1)} %pad_maximum_fusion.1.kv_ref, bf16[128,512]{1,0:T(8,128)(2,1)} %og_ref.1, f32[8,128]{1,0:T(8,128)} %pad.4.g_ref, f32[1,512]{1,0:T(1,128)} %bitcast.15, ...), custom_call_target="tpu_custom_call" | custom-call | tf_op jit(solution)/shard_map/pallas_call | solution.py:546
  139.0 1.6 %copy.17 = bf16[128,512]{1,0:T(8,128)(2,1)} copy(bf16[128,512]{1,0:T(8,128)(2,1)} %shard_map.127) | data formatting | bytes 262144
  (1 shorter events, 0.0 us)
Async XLA Ops:
  1.4 2.7 %copy-start = (bf16[128,512]{1,0:T(8,128)(2,1)S(1)}, bf16[128,512]{1,0:T(8,128)(2,1)}, u32[]{:S(2)}) copy-start(bf16[128,512]{1,0:T(8,128)(2,1)} %param.16) | copy-start | bytes 393220
  1.4 2.7 %copy-start.1 = (bf16[128,256]{1,0:T(8,128)(2,1)S(1)}, bf16[128,256]{1,0:T(8,128)(2,1)}, u32[]{:S(2)}) copy-start(bf16[128,256]{1,0:T(8,128)(2,1)} %param.15) | copy-start | bytes 196612
  1.4 3.4 %copy-start.2 = (f32[128,2]{0,1:T(2,128)S(1)}, f32[128,2]{0,1:T(2,128)}, u32[]{:S(2)}) copy-start(f32[128,2]{0,1:T(2,128)} %param.18) | copy-start | bytes 3076
  1.4 3.4 %copy-start.3 = (f32[128,2]{0,1:T(2,128)S(1)}, f32[128,2]{0,1:T(2,128)}, u32[]{:S(2)}) copy-start(f32[128,2]{0,1:T(2,128)} %param.19) | copy-start | bytes 3076

commit v2 on v1

--- a/solution.py
+++ b/solution.py
@@ -292,8 +292,6 @@
         kv_forward(r).start()
     for r in range(1, n, 2):
         gu_copy(r).start()
-    for r in range(1, n):
-        d_copy(r).start()
     for r in range(1, n):
         g_copy(r).wait_recv()
     for r in range(1, n, 2):
@@ -393,6 +391,8 @@
 
     for r in direct:
         x_copy(r).start()
+    for r in range(2, n, 2):
+        d_copy(r).start()
     order = [0] + [r for base in range(2, n, 2) for r in (base, base + 1)] + [1]
     for i in range(n + levels):
         if i < n:
@@ -403,6 +403,9 @@
                 x_forward(r).start()
             for j in range(share(levels - 1)):
                 xt_copy(levels - 1, r, j).start()
+        if i == n - 2:
+            for r in range(1, n, 2):
+                d_copy(r).start()
         for back in range(1, levels + 1):
             if 0 <= i - back < n:
                 r, level = order[i - back], levels - back
@@ -413,8 +416,6 @@
                         xt_copy(level - 1, r, j).start()
     for r in range(1, n):
         gu_copy(r).wait_recv()
-    for r in range(1, n):
-        d_copy(r).wait_recv()
 
     part, depth = wdb.shape[1], wgub.shape[2]
     nt = (((1,), (1,)), ((), ()))
@@ -445,6 +446,12 @@
                     normed, wgub[k, part:], nt, preferred_element_type=jnp.float32
                 )
             hidden = (gate_act / (1.0 + jnp.exp(-gate_act)) * up_act).astype(jnp.bfloat16)
+
+            @pl.when(i == 0)
+            def _():
+                for r in range(1, n):
+                    d_copy(r).wait_recv()
+
             for k in range(n):
                 j, c = k // per, (k % per) * depth
                 ob[b, j, :, c : c + depth] = jnp.dot(

time: 141 us -> 132 us (0.936)
  Pallas kernels: 134 us -> 124 us
    pallas_call x1, Pallas kernels: 134 us -> 124 us  [fused(): pl.pallas_call(functools.partial(fused_kernel, n, m, heads), out_shape=ja...]
where the time goes in v2:
time: 132 us; the launch traced here: 131 us
  Pallas kernels  124 us (94%)
  local copies, waits for them, and re-layouts  5.03 us (4%)
  other arithmetic  1.91 us (1%)
    pallas_call x1, Pallas kernels, fused(): pl.pallas_call(functools.partial(fused_kernel, n, m, heads), out_shape=ja...  124 us
    transpose x2, local copies, waits for them, and re-layouts, fused(): flip = lambda w: w.T.reshape(n, part, depth)  2.84 us

profile of v2, /device:TPU:0, one launch (start us, length us, event | category | flops | bytes accessed | tf_op | source)
XLA Modules:
  0.0 131.5 jit_solution(8981835468730744994)
XLA Ops:
  0.0 1.4 %copy.14 = bf16[1408,256]{1,0:T(8,128)(2,1)S(1)} copy(bf16[1408,256]{0,1:T(8,128)(2,1)} %bitcast.11) | data formatting | bytes 1441792 | tf_op jit(solution)/shard_map/transpose | solution.py:540
  1.4 0.0 copy-start
  1.4 0.0 copy-start.1
  1.4 0.0 copy-start.2
  1.4 0.0 copy-start.3
  1.4 1.5 %copy.15 = bf16[1408,256]{1,0:T(8,128)(2,1)S(1)} copy(bf16[1408,256]{0,1:T(8,128)(2,1)} %bitcast.12) | data formatting | bytes 1441792 | tf_op jit(solution)/shard_map/transpose | solution.py:540
  2.9 1.2 pad_maximum_fusion.wgu_ref
  4.1 0.0 copy-done
  4.1 0.0 copy-done.1
  4.1 0.7 pad_maximum_fusion.1.kv_ref
  4.8 0.0 copy-done.2
  4.8 0.0 copy-done.3
  4.8 0.6 pad.4.g_ref
  5.4 124.5 %shard_map.127 = bf16[128,512]{1,0:T(8,128)(2,1)} custom-call(bf16[128,512]{1,0:T(8,128)(2,1)} %stream_ref.1, bf16[128,256]{1,0:T(8,128)(2,1)} %q_ref.1, bf16[128,768]{1,0:T(8,128)(2,1)} %pad_maximum_fusion.1.kv_ref, bf16[128,512]{1,0:T(8,128)(2,1)} %og_ref.1, f32[8,128]{1,0:T(8,128)} %pad.4.g_ref, f32[1,512]{1,0:T(1,128)} %bitcast.15, ...), custom_call_target="tpu_custom_call" | custom-call | tf_op jit(solution)/shard_map/pallas_call | solution.py:553
  129.9 1.6 %copy.17 = bf16[128,512]{1,0:T(8,128)(2,1)} copy(bf16[128,512]{1,0:T(8,128)(2,1)} %shard_map.127) | data formatting | bytes 262144
  (1 shorter events, 0.0 us)
Async XLA Ops:
  1.4 2.7 %copy-start = (bf16[128,512]{1,0:T(8,128)(2,1)S(1)}, bf16[128,512]{1,0:T(8,128)(2,1)}, u32[]{:S(2)}) copy-start(bf16[128,512]{1,0:T(8,128)(2,1)} %param.16) | copy-start | bytes 393220
  1.4 2.7 %copy-start.1 = (bf16[128,256]{1,0:T(8,128)(2,1)S(1)}, bf16[128,256]{1,0:T(8,128)(2,1)}, u32[]{:S(2)}) copy-start(bf16[128,256]{1,0:T(8,128)(2,1)} %param.15) | copy-start | bytes 196612
  1.4 3.4 %copy-start.2 = (f32[128,2]{0,1:T(2,128)S(1)}, f32[128,2]{0,1:T(2,128)}, u32[]{:S(2)}) copy-start(f32[128,2]{0,1:T(2,128)} %param.18) | copy-start | bytes 3076
  1.4 3.4 %copy-start.3 = (f32[128,2]{0,1:T(2,128)S(1)}, f32[128,2]{0,1:T(2,128)}, u32[]{:S(2)}) copy-start(f32[128,2]{0,1:T(2,128)} %param.19) | copy-start | bytes 3076

commit v3 on v2

--- a/solution.py
+++ b/solution.py
@@ -290,8 +290,6 @@
     for r in range(2, n, 2):
         kv_copy(r).wait_recv()
         kv_forward(r).start()
-    for r in range(1, n, 2):
-        gu_copy(r).start()
     for r in range(1, n):
         g_copy(r).wait_recv()
     for r in range(1, n, 2):
@@ -391,8 +389,6 @@
 
     for r in direct:
         x_copy(r).start()
-    for r in range(2, n, 2):
-        d_copy(r).start()
     order = [0] + [r for base in range(2, n, 2) for r in (base, base + 1)] + [1]
     for i in range(n + levels):
         if i < n:
@@ -401,10 +397,12 @@
                 x_copy(r).wait_recv()
             if r and r % 2 == 0:
                 x_forward(r).start()
+                gu_copy(r + 1).start()
             for j in range(share(levels - 1)):
                 xt_copy(levels - 1, r, j).start()
         if i == n - 2:
-            for r in range(1, n, 2):
+            gu_copy(1).start()
+            for r in range(1, n):
                 d_copy(r).start()
         for back in range(1, levels + 1):
             if 0 <= i - back < n:

time: 132 us -> 140 us (1.061)
  Pallas kernels: 124 us -> 133 us
    pallas_call x1, Pallas kernels: 124 us -> 133 us  [fused(): pl.pallas_call(functools.partial(fused_kernel, n, m, heads), out_shape=ja...]
where the time goes in v3:
time: 140 us
  Pallas kernels  133 us (95%)
  local copies, waits for them, and re-layouts  5.03 us (4%)
  other arithmetic  1.91 us (1%)
    pallas_call x1, Pallas kernels, fused(): pl.pallas_call(functools.partial(fused_kernel, n, m, heads), out_shape=ja...  133 us
    transpose x2, local copies, waits for them, and re-layouts, fused(): flip = lambda w: w.T.reshape(n, part, depth)  2.84 us

profile of v3, /device:TPU:0, one launch (start us, length us, event | category | flops | bytes accessed | tf_op | source)
XLA Modules:
  0.0 139.6 jit_solution(11135202977093618917)
XLA Ops:
  0.0 1.4 copy.14
  1.4 0.0 copy-start
  1.4 0.0 copy-start.1
  1.4 0.0 copy-start.2
  1.4 0.0 copy-start.3
  1.4 1.5 %copy.15 = bf16[1408,256]{1,0:T(8,128)(2,1)S(1)} copy(bf16[1408,256]{0,1:T(8,128)(2,1)} %bitcast.12) | data formatting | bytes 1441792 | tf_op jit(solution)/shard_map/transpose | solution.py:538
  2.9 1.2 pad_maximum_fusion.wgu_ref
  4.1 0.0 copy-done
  4.1 0.0 copy-done.1
  4.1 0.7 pad_maximum_fusion.1.kv_ref
  4.8 0.0 copy-done.2
  4.8 0.0 copy-done.3
  4.8 0.6 pad.4.g_ref
  5.4 132.6 %shard_map.127 = bf16[128,512]{1,0:T(8,128)(2,1)} custom-call(bf16[128,512]{1,0:T(8,128)(2,1)} %stream_ref.1, bf16[128,256]{1,0:T(8,128)(2,1)} %q_ref.1, bf16[128,768]{1,0:T(8,128)(2,1)} %pad_maximum_fusion.1.kv_ref, bf16[128,512]{1,0:T(8,128)(2,1)} %og_ref.1, f32[8,128]{1,0:T(8,128)} %pad.4.g_ref, f32[1,512]{1,0:T(1,128)} %bitcast.15, ...), custom_call_target="tpu_custom_call" | custom-call | tf_op jit(solution)/shard_map/pallas_call | solution.py:551
  138.0 1.6 %copy.17 = bf16[128,512]{1,0:T(8,128)(2,1)} copy(bf16[128,512]{1,0:T(8,128)(2,1)} %shard_map.127) | data formatting | bytes 262144
  (1 shorter events, 0.0 us)
Async XLA Ops:
  1.4 2.7 %copy-start = (bf16[128,512]{1,0:T(8,128)(2,1)S(1)}, bf16[128,512]{1,0:T(8,128)(2,1)}, u32[]{:S(2)}) copy-start(bf16[128,512]{1,0:T(8,128)(2,1)} %param.16) | copy-start | bytes 393220
  1.4 2.7 %copy-start.1 = (bf16[128,256]{1,0:T(8,128)(2,1)S(1)}, bf16[128,256]{1,0:T(8,128)(2,1)}, u32[]{:S(2)}) copy-start(bf16[128,256]{1,0:T(8,128)(2,1)} %param.15) | copy-start | bytes 196612
  1.4 3.4 %copy-start.2 = (f32[128,2]{0,1:T(2,128)S(1)}, f32[128,2]{0,1:T(2,128)}, u32[]{:S(2)}) copy-start(f32[128,2]{0,1:T(2,128)} %param.18) | copy-start | bytes 3076
  1.4 3.4 %copy-start.3 = (f32[128,2]{0,1:T(2,128)S(1)}, f32[128,2]{0,1:T(2,128)}, u32[]{:S(2)}) copy-start(f32[128,2]{0,1:T(2,128)} %param.19) | copy-start | bytes 3076
